TPU v7x, 512 devices: a whole 4x8x8 slice. The times are simulated.
512 devices in a mesh: sp: 32 (over z, x), dp: 16 (over y, core).
Axes of the slice: x: 4, y: 8, z: 8, core: 2. Of those that a mesh axis runs over, the one named last changes fastest.
Arguments:
- tokens: bfloat16 [16, 16384, 2048], P('dp', 'sp'), may hold values from -6 to 6
- segments: int32 [16, 16384], P('dp', 'sp'), may hold values from 0 to 15, never falling along the last dimension, each value on 1 to 2048 neighbouring positions
- w_lin: bfloat16 [2048, 1024], P('dp'), may hold values from -0.125 to 0.125
- w_gate: bfloat16 [2048, 1024], P('dp'), may hold values from -0.125 to 0.125
- w_out: bfloat16 [1024, 2048], P(None, 'dp'), may hold values from -0.1875 to 0.1875
- conv_kernel: float32 [31, 1024], replicated, may hold values from -1 to 1
- conv_bias: float32 [1024], replicated, may hold values from -3 to 3
- norm_gain: float32 [1024], replicated, may hold values from 0.1 to 1.9
- norm_bias: float32 [1024], replicated, may hold values from -3 to 3
Outputs:
- mixed_out: bfloat16 [16, 16384, 2048], P('dp', 'sp')
Inputs may be any that keep to these rules, and one draw needn't show every extreme that they name: `segments`: within each sequence document numbers never fall; a document is a run of equal numbers of at most four times 512 positions.
All inputs are finite; a program needn't handle non-finite values.
Results may differ from a plain program's by a relative error of at most 0.0062.
Values may be sent and summed in bfloat16 or wider, within the bound.
A program may use at most 64 MiB of HBM per device.

v0:
```python
import jax
import jax.numpy as jnp
from jax import lax
from jax.sharding import PartitionSpec as P

K = 31


def sent_together(arrays, axis, dim, along):
    both = jnp.concatenate(arrays, axis=along)
    result, at, outs = (lax.all_gather(both, axis, axis=dim, tiled=True), 0, [])
    for a in arrays:
        outs.append(lax.slice_in_dim(result, at, at + a.shape[along], axis=along))
        at += a.shape[along]
    return tuple(outs)


def from_behind(value, axis, by):
    devices = lax.axis_size(axis)
    pairs = [(i, i + by) for i in range(devices) if 0 <= i + by < devices]
    return lax.ppermute(value, axis, pairs)


def conv_doc(values, doc_ids, kernel, bias):
    taps = kernel.shape[0]
    reach = taps - 1
    length = values.shape[1]
    place = lax.iota(jnp.int32, length)
    change = jnp.concatenate([jnp.ones((1,), jnp.bool_), doc_ids[1:] != doc_ids[:-1]])
    begins = lax.cummax(jnp.where(change, place, 0), axis=0)[reach:]
    here = place[reach:]
    total = bias[:, None] + kernel[reach][:, None] * values[:, reach:].astype(jnp.float32)
    for back in range(1, taps):
        piece = values[:, reach - back : length - back].astype(jnp.float32)
        keep = here - back >= begins
        total = total + kernel[reach - back][:, None] * jnp.where(keep[None, :], piece, 0.0)
    return total


def body(tokens, segments, w_lin, w_gate, w_out, conv_kernel, conv_bias, norm_gain, norm_bias):
    rows = tokens[0]
    doc_ids = segments[0]
    count = rows.shape[0]
    reach = K - 1
    pieces = sent_together((w_lin, w_gate), "dp", 0, 1)
    first = jnp.einsum("rc,tr->ct", pieces[0], rows, preferred_element_type=jnp.float32)
    second = jnp.einsum("rc,tr->ct", pieces[1], rows, preferred_element_type=jnp.float32)
    glu = (first * jax.nn.sigmoid(second)).astype(jnp.bfloat16)
    tail, tail_ids = from_behind((glu[:, count - reach :], doc_ids[count - reach :]), "sp", 1)
    extended = jnp.concatenate([tail, glu], axis=1)
    ext_ids = jnp.concatenate([tail_ids, doc_ids], axis=0)
    conv = conv_doc(extended, ext_ids, conv_kernel, conv_bias)
    conved = lax.optimization_barrier(conv.astype(jnp.bfloat16))
    values = conved.astype(jnp.float32)
    mean = jnp.mean(values, axis=0, keepdims=True)
    var = jnp.mean(jnp.square(values - mean), axis=0, keepdims=True)
    normed = (values - mean) * lax.rsqrt(var + 1e-05) * norm_gain[:, None] + norm_bias[:, None]
    act = jax.nn.silu(normed).astype(jnp.bfloat16)
    mixed_out = jnp.einsum(
        "ct,cr->tr",
        act,
        lax.all_gather(w_out, "dp", axis=1, tiled=True),
        preferred_element_type=jnp.float32,
    ).astype(jnp.bfloat16)
    return mixed_out[None]


def solution(mesh):
    placed = (
        P("dp", "sp", None),
        P("dp", "sp"),
        P("dp", None),
        P("dp", None),
        P(None, "dp"),
        P(),
        P(),
        P(),
        P(),
    )
    return jax.shard_map(
        body, mesh=mesh, in_specs=placed, out_specs=P("dp", "sp", None), check_vma=False
    )
```

profile of v0, /device:TPU:1, one launch (start us, length us, event | category | flops | bytes accessed | tf_op | source)
XLA Modules:
  0.0 140.4 jit_solution(699867994584362061)
XLA Ops:
  6.5 0.0 copy-start
  6.5 0.0 copy-start.2
  6.5 0.0 all-gather.3.cloned.1.call-start
  6.5 2.0 %pad_maximum_fusion.1 = bf16[128,2048]{1,0:T(8,128)(2,1)} fusion(bf16[128,1024]{1,0:T(8,128)(2,1)} %param.12, bf16[128,1024]{1,0:T(8,128)(2,1)} %param.11), kind=kLoop, calls=%fused_computation.92 | loop fusion | flops 1048576 | bytes 1048576 | tf_op jit(solution)/shard_map/concatenate | solution.py:10
  8.6 0.0 all-gather.3.cloned.1.call-update
  8.6 0.0 all-gather.5.cloned.1.call-start
  8.6 0.7 all-gather.5.cloned.1.call-update
  9.3 0.7 slice_bitcast_fusion
  10.1 3.9 %collective-permute-start = (s32[30]{0:T(128)S(1)}, s32[30]{0:T(128)S(1)}, u32[]{:S(2)}, u32[]{:S(2)}) collective-permute-start(s32[30]{0:T(128)S(1)} %slice_bitcast_fusion), channel_id=1, source_target_pairs={{0,16},{16,32},{32,48},{48,64},{64,80},{80,96},{96,112},{112,128},... | collective-permute-start | bytes 368 | tf_op jit(solution)/shard_map/ppermute | solution.py:21
  14.0 1.4 fusion.58
  15.4 1.1 fusion.59
  16.5 0.0 collective-permute-done
  16.5 0.0 copy-done.2
  16.5 0.1 pad_add_fusion
  16.6 0.1 slice_compare_fusion
  16.7 0.1 iota_select_fusion
  16.8 0.3 reduce-window.9
  17.0 0.1 slice.286
  17.1 0.1 slice_reduce_fusion
  17.3 0.1 maximum_bitcast_fusion
  17.3 0.1 add_compare_fusion.29
  17.4 0.1 add_compare_fusion.20
  17.5 0.1 add_compare_fusion.11
  17.6 55.9 %all-gather.3.cloned.1.call-done = bf16[2048,2048]{1,0:T(8,128)(2,1)} async-done(((bf16[128,2048]{1,0:T(8,128)(2,1)}), bf16[2048,2048]{1,0:T(8,128)(2,1)}) %all-gather.3.cloned.1.call-update) | async-done | bytes 8388624 | tf_op jit(solution)/shard_map/all_gather | solution.py:11
  73.5 0.0 copy-done
  73.5 0.0 copy-start.3
  73.5 4.7 %fusion = f32[1024,512]{0,1:T(8,128)S(1)} fusion(bf16[2048,2048]{1,0:T(8,128)(2,1)} %all-gather.3.cloned.1.call-done, bf16[1,512,2048]{2,1,0:T(8,128)(2,1)S(1)} %copy-done), kind=kOutput, calls=%fused_computation.29 | convolution fusion | flops 2147483648 | bytes 8388608 | tf_op jit(solution)/shard_map/rc,tr->ct/dot_general | solution.py:47
  78.2 0.0 copy-done.3
  78.2 0.0 copy-start.1
  78.2 2.5 %multiply_convert_fusion = bf16[1024,512]{0,1:T(8,128)(2,1)S(1)} fusion(f32[1024,512]{0,1:T(8,128)S(1)} %fusion, bf16[2048,2048]{1,0:T(8,128)(2,1)S(1)} %copy-done.3, bf16[1,512,2048]{2,1,0:T(8,128)(2,1)S(1)} %copy-done), kind=kOutput, calls=%fused_computation.51 | convolution fusion | flops 2150105088 | bytes 9437184 | tf_op jit(solution)/shard_map/rc,tr->ct/dot_general | solution.py:46
  80.7 3.1 %collective-permute-start.1 = (bf16[1024,30]{0,1:T(8,128)(2,1)S(1)}, bf16[1024,30]{0,1:T(8,128)(2,1)S(1)}, u32[]{:S(2)}, u32[]{:S(2)}) collective-permute-start(bf16[1024,30]{0,1:T(8,128)(2,1)S(1)} %slice.351), channel_id=1, source_target_pairs={{0,16},{16,32},{32,48},{48,64},{64,80},{80,96},{96,112},{112,128},... | collective-permute-start | bytes 184328 | tf_op jit(solution)/shard_map/ppermute | solution.py:21
  83.8 0.1 add_compare_fusion.2
  83.9 1.2 collective-permute-done.1
  85.2 0.0 copy-done.1
  85.2 0.0 copy-start.4
  85.2 0.0 copy-start.5
  85.2 15.9 %add_convert_fusion = bf16[1024,512]{0,1:T(8,128)(2,1)S(1)} fusion(bf16[1024,512]{0,1:T(8,128)(2,1)S(1)} %multiply_convert_fusion, bf16[1024,30]{0,1:T(8,128)(2,1)S(1)} %collective-permute-done.1, f32[1024]{0:T(1024)S(1)} %bitcast.77, f32[1024]{0:T(1024)S(1)} %bitcast.78, f32[1024]{0:T(1024)S(1)} %bitcast.49, f32[1024]{0:T(1024)S(1)} %bitcast.50, ...), kind=kLoop, calls=%fused_computation.50 | loop fusion | flops 112197632 | bytes 2305024 | tf_op jit(solution)/shard_map/convert_element_type | solution.py:53
  101.0 0.2 convert_reduce_fusion
  101.3 0.4 fusion.7
  101.7 25.5 %all-gather.5.cloned.1.call-done = bf16[1024,2048]{1,0:T(8,128)(2,1)} async-done(((bf16[1024,128]{1,0:T(8,128)(2,1)}), bf16[1024,2048]{1,0:T(8,128)(2,1)}) %all-gather.5.cloned.1.call-update) | async-done | bytes 4194320 | tf_op jit(solution)/shard_map/all_gather | solution.py:62
  127.2 0.0 copy-done.4
  127.2 0.0 copy-done.5
  127.2 6.4 %fusion.4 = bf16[1,512,2048]{2,1,0:T(8,128)(2,1)} fusion(bf16[1024,2048]{1,0:T(8,128)(2,1)} %all-gather.5.cloned.1.call-done, bf16[1024,512]{0,1:T(8,128)(2,1)S(1)} %add_convert_fusion, f32[1024]{0:T(1024)S(1)} %copy-done.4, f32[1024]{0:T(1024)S(1)} %copy-done.5, f32[512]{0:T(512)S(1)} %add_rsqrt_fusion, f32[512]{0:T(512)S(1)} %broadcast_multiply_fusion), kind=kOutput, calls=%fused_computation.34 | convolution fusion | flops 2153775104 | bytes 7352320 | tf_op jit(solution)/shard_map/ct,cr->tr/dot_general | solution.py:59
  (6 shorter events, 0.1 us)
Async XLA Ops:
  6.5 67.0 %copy-start = (bf16[1,512,2048]{2,1,0:T(8,128)(2,1)S(1)}, bf16[1,512,2048]{2,1,0:T(8,128)(2,1)}, u32[]{:S(2)}) copy-start(bf16[1,512,2048]{2,1,0:T(8,128)(2,1)} %param.9) | copy-start | bytes 6291460
  6.5 10.0 %copy-start.2 = (s32[1,512]{1,0:T(1,128)S(1)}, s32[1,512]{1,0:T(1,128)}, u32[]{:S(2)}) copy-start(s32[1,512]{1,0:T(1,128)} %param.10) | copy-start | bytes 6148
  6.5 67.0 %all-gather.3.cloned.1.call-start = ((), (), s32[]{:S(2)}) async-start(), calls=%async_computation | async-start | bytes 8912896 | tf_op jit(solution)/shard_map/all_gather | solution.py:11
  8.6 118.6 %all-gather.5.cloned.1.call-start = ((), (), s32[]{:S(2)}) async-start(), calls=%async_computation.1 | async-start | bytes 4456448 | tf_op jit(solution)/shard_map/all_gather | solution.py:62
  10.1 6.4 %collective-permute-start = (s32[30]{0:T(128)S(1)}, s32[30]{0:T(128)S(1)}, u32[]{:S(2)}, u32[]{:S(2)}) collective-permute-start(s32[30]{0:T(128)S(1)} %slice_bitcast_fusion), channel_id=1, source_target_pairs={{0,16},{16,32},{32,48},{48,64},{64,80},{80,96},{96,112},{112,128},... | collective-permute-start | bytes 368 | tf_op jit(solution)/shard_map/ppermute | solution.py:21
  73.5 4.7 %copy-start.3 = (bf16[2048,2048]{1,0:T(8,128)(2,1)S(1)}, bf16[2048,2048]{1,0:T(8,128)(2,1)}, u32[]{:S(2)}) copy-start(bf16[2048,2048]{1,0:T(8,128)(2,1)} %all-gather.3.cloned.1.call-done) | copy-start | bytes 25165828
  78.2 7.0 %copy-start.1 = (f32[1024]{0:T(1024)S(1)}, f32[1024]{0:T(1024)}, u32[]{:S(2)}) copy-start(f32[1024]{0:T(1024)} %param.15) | copy-start | bytes 12292
  80.7 4.4 %collective-permute-start.1 = (bf16[1024,30]{0,1:T(8,128)(2,1)S(1)}, bf16[1024,30]{0,1:T(8,128)(2,1)S(1)}, u32[]{:S(2)}, u32[]{:S(2)}) collective-permute-start(bf16[1024,30]{0,1:T(8,128)(2,1)S(1)} %slice.351), channel_id=1, source_target_pairs={{0,16},{16,32},{32,48},{48,64},{64,80},{80,96},{96,112},{112,128},... | collective-permute-start | bytes 184328 | tf_op jit(solution)/shard_map/ppermute | solution.py:21
  85.2 42.0 %copy-start.4 = (f32[1024]{0:T(1024)S(1)}, f32[1024]{0:T(1024)}, u32[]{:S(2)}) copy-start(f32[1024]{0:T(1024)} %param.17) | copy-start | bytes 12292
  85.2 42.0 %copy-start.5 = (f32[1024]{0:T(1024)S(1)}, f32[1024]{0:T(1024)}, u32[]{:S(2)}) copy-start(f32[1024]{0:T(1024)} %param.16) | copy-start | bytes 12292
Sparse Core Ops, SparseCore 0:
  9.5 64.0 all-gather.2
  75.6 51.5 all-gather.4
where the time goes:
time: 141 us; the launch traced here: 140 us
  waiting for transfers between devices  83.4 us (59%)
  other arithmetic  19.5 us (14%)
  matrix products  13.5 us (10%)
  between operations  13.5 us (10%)
  starting transfers between devices  7.06 us (5%)
  local copies, waits for them, and re-layouts  3.47 us (2%)
    all_gather x1, waiting for transfers between devices, sent_together(): result, at, outs = (lax.all_gather(both, axis, axis=dim, tiled=True), 0, [])  55.9 us
    all_gather x1, waiting for transfers between devices, body(): lax.all_gather(w_out, 'dp', axis=1, tiled=True)  25.5 us
    convert_element_type x1, other arithmetic, body(): conved = lax.optimization_barrier(conv.astype(jnp.bfloat16))  15.9 us
    ppermute x2, starting transfers between devices, from_behind(): return lax.ppermute(value, axis, pairs)  7.01 us
    dot_general x1, matrix products, body(): jnp.einsum('ct,cr->tr', act, lax.all_gather(w_out, 'dp', axis=1, tiled=Tr...  6.35 us
    dot_general x1, matrix products, body(): jnp.einsum('rc,tr->ct', pieces[1], rows, preferred_element_type=jnp.float32)  4.66 us
  transfers between devices with their start and end apart: 4, of which 3 were waited for; matrix products, arithmetic and copies ran while one was open for 20% of the time, Pallas kernels for 0%

commit v1 on v0

--- a/solution.py
+++ b/solution.py
@@ -4,6 +4,11 @@
 from jax.sharding import PartitionSpec as P
 
 K = 31
+
+
+def tiled_gather(x, axis, dim):
+    copies = jnp.concatenate([x] * lax.axis_size(axis), axis=dim)
+    return lax.all_to_all(copies, axis, dim, dim, tiled=True)
 
 
 def sent_together(arrays, axis, dim, along):
@@ -57,10 +62,7 @@
     normed = (values - mean) * lax.rsqrt(var + 1e-05) * norm_gain[:, None] + norm_bias[:, None]
     act = jax.nn.silu(normed).astype(jnp.bfloat16)
     mixed_out = jnp.einsum(
-        "ct,cr->tr",
-        act,
-        lax.all_gather(w_out, "dp", axis=1, tiled=True),
-        preferred_element_type=jnp.float32,
+        "ct,cr->tr", act, tiled_gather(w_out, "dp", 1), preferred_element_type=jnp.float32
     ).astype(jnp.bfloat16)
     return mixed_out[None]
 

time: 141 us -> 207 us (1.47)
  waiting for transfers between devices: 83.4 us -> 131 us
  local copies, waits for them, and re-layouts: 3.47 us -> 16.5 us
  starting transfers between devices: 7.06 us -> 14.6 us
  matrix products: 13.5 us -> 11.3 us
    all_gather x1, waiting for transfers between devices: 55.9 us -> 131 us  [sent_together(): result, at, outs = (lax.all_gather(both, axis, axis=dim, tiled=True), 0, [])]
    all_gather x1 -> x0, waiting for transfers between devices: 25.5 us -> none  [body(): lax.all_gather(w_out, 'dp', axis=1, tiled=True)]
    all_to_all x0 -> x2, local copies, waits for them, and re-layouts: none -> 12.7 us  [tiled_gather(): return lax.all_to_all(copies, axis, dim, dim, tiled=True)]
    all_to_all x0 -> x1, starting transfers between devices: none -> 11.3 us  [tiled_gather(): return lax.all_to_all(copies, axis, dim, dim, tiled=True)]
    ppermute x2, starting transfers between devices: 7.01 us -> 3.34 us  [from_behind(): return lax.ppermute(value, axis, pairs)]
    unnamed x12 -> x34, local copies, waits for them, and re-layouts: 0.03 us -> 3.37 us
    dot_general x1, matrix products: 6.35 us -> 4.2 us  [body(): jnp.einsum('ct,cr->tr', act, tiled_gather(w_out, 'dp', 1), preferred_elem...]
  transfers between devices with their start and end apart: 4 -> 4, of which waited for: 3 -> 2; matrix products, arithmetic and copies ran while one was open for 20% -> 11% of each run, Pallas kernels for 0% -> 0%
where the time goes in v1:
time: 207 us
  waiting for transfers between devices  131 us (63%)
  other arithmetic  19.7 us (10%)
  local copies, waits for them, and re-layouts  16.5 us (8%)
  starting transfers between devices  14.6 us (7%)
  between operations  13.7 us (7%)
  matrix products  11.3 us (5%)
    all_gather x1, waiting for transfers between devices, sent_together(): result, at, outs = (lax.all_gather(both, axis, axis=dim, tiled=True), 0, [])  131 us
    convert_element_type x1, other arithmetic, body(): conved = lax.optimization_barrier(conv.astype(jnp.bfloat16))  16.1 us
    all_to_all x2, local copies, waits for them, and re-layouts, tiled_gather(): return lax.all_to_all(copies, axis, dim, dim, tiled=True)  12.7 us
    all_to_all x1, starting transfers between devices, tiled_gather(): return lax.all_to_all(copies, axis, dim, dim, tiled=True)  11.3 us
    dot_general x1, matrix products, body(): jnp.einsum('rc,tr->ct', pieces[1], rows, preferred_element_type=jnp.float32)  4.66 us
    dot_general x1, matrix products, body(): jnp.einsum('ct,cr->tr', act, tiled_gather(w_out, 'dp', 1), preferred_elem...  4.2 us
  transfers between devices with their start and end apart: 4, of which 2 were waited for; matrix products, arithmetic and copies ran while one was open for 11% of the time, Pallas kernels for 0%

profile of v1, /device:TPU:1, one launch (start us, length us, event | category | flops | bytes accessed | tf_op | source)
XLA Modules:
  0.0 206.9 jit_solution(9880313048619763233)
XLA Ops:
  6.5 0.0 copy-start
  6.5 0.0 all-gather.2.cloned.1.call-start
  6.5 2.0 pad_maximum_fusion.1
  8.6 0.0 all-gather.2.cloned.1.call-update
  8.6 1.1 copy.10
  10.1 0.0 copy-start.1
  10.1 2.0 copy-done.1
  12.1 6.3 %copy.26 = bf16[1024,16,128]{2,0,1:T(8,128)(2,1)} copy(bf16[1024,16,128]{0,2,1:T(8,128)(2,1)} %bitcast.50) | data formatting | bytes 8388608 | tf_op jit(solution)/shard_map/all_to_all | solution.py:11
  18.4 0.0 copy-start.5
  18.4 0.0 copy-start.3
  18.4 11.3 %all-to-all-start = ((bf16[1024,16,128]{2,0,1:T(8,128)(2,1)}), bf16[1024,16,128]{2,0,1:T(8,128)(2,1)}, u32[]{:S(2)}, u32[]{:S(2)}) async-start(bf16[1024,16,128]{2,0,1:T(8,128)(2,1)} %copy.26), calls=%async_computation | async-start | bytes 8388608 | tf_op jit(solution)/shard_map/all_to_all | solution.py:11
  29.7 0.0 copy-done.5
  29.7 0.1 slice_bitcast_fusion
  29.8 1.3 collective-permute-start
  31.0 0.0 copy-done.3
  31.0 0.1 fusion.58
  31.2 0.6 collective-permute-done
  31.7 0.1 pad_add_fusion
  31.8 0.1 slice_compare_fusion
  31.9 0.1 iota_select_fusion
  32.0 0.3 reduce-window.9
  32.3 0.1 slice.286
  32.4 0.1 slice_reduce_fusion
  32.5 0.1 maximum_bitcast_fusion
  32.6 0.1 add_compare_fusion.20
  32.6 0.1 add_compare_fusion.11
  32.7 0.1 add_compare_fusion.29
  32.8 130.6 %all-gather.2.cloned.1.call-done = bf16[2048,2048]{1,0:T(8,128)(2,1)} async-done(((bf16[128,2048]{1,0:T(8,128)(2,1)}), bf16[2048,2048]{1,0:T(8,128)(2,1)}) %all-gather.2.cloned.1.call-update) | async-done | bytes 8388624 | tf_op jit(solution)/shard_map/all_gather | solution.py:16
  163.4 0.0 copy-done
  163.4 0.0 copy-start.6
  163.4 4.7 %fusion = f32[1024,512]{0,1:T(8,128)S(1)} fusion(bf16[2048,2048]{1,0:T(8,128)(2,1)} %all-gather.2.cloned.1.call-done, bf16[1,512,2048]{2,1,0:T(8,128)(2,1)S(1)} %copy-done), kind=kOutput, calls=%fused_computation.29 | convolution fusion | flops 2147483648 | bytes 8388608 | tf_op jit(solution)/shard_map/rc,tr->ct/dot_general | solution.py:52
  168.1 0.0 copy-done.6
  168.1 2.4 %multiply_convert_fusion = bf16[1024,512]{0,1:T(8,128)(2,1)S(1)} fusion(f32[1024,512]{0,1:T(8,128)S(1)} %fusion, bf16[2048,2048]{1,0:T(8,128)(2,1)S(1)} %copy-done.6, bf16[1,512,2048]{2,1,0:T(8,128)(2,1)S(1)} %copy-done), kind=kOutput, calls=%fused_computation.51 | convolution fusion | flops 2150105088 | bytes 9437184 | tf_op jit(solution)/shard_map/rc,tr->ct/dot_general | solution.py:51
  170.5 2.1 collective-permute-start.1
  172.6 0.1 add_compare_fusion.2
  172.7 0.0 copy-start.4
  172.7 0.0 all-to-all-done
  172.7 6.4 %copy.27 = bf16[1024,16,128]{0,2,1:T(8,128)(2,1)} copy(bf16[1024,16,128]{2,0,1:T(8,128)(2,1)} %all-to-all-done) | data formatting | bytes 8388608 | tf_op jit(solution)/shard_map/all_to_all | solution.py:11
  179.1 0.0 collective-permute-done.1
  179.1 0.0 copy-done.4
  179.1 0.0 copy-start.2
  179.1 0.0 copy-start.7
  179.1 0.0 copy-start.8
  179.1 16.1 %add_convert_fusion = bf16[1024,512]{0,1:T(8,128)(2,1)S(1)} fusion(bf16[1024,512]{0,1:T(8,128)(2,1)S(1)} %multiply_convert_fusion, bf16[1024,30]{0,1:T(8,128)(2,1)S(1)} %collective-permute-done.1, f32[1024]{0:T(1024)S(1)} %bitcast.81, f32[1024]{0:T(1024)S(1)} %bitcast.82, f32[1024]{0:T(1024)S(1)} %bitcast.53, f32[1024]{0:T(1024)S(1)} %bitcast.54, ...), kind=kLoop, calls=%fused_computation.50 | loop fusion | flops 112197632 | bytes 2305024 | tf_op jit(solution)/shard_map/convert_element_type | solution.py:58
  195.2 0.2 convert_reduce_fusion
  195.4 0.4 fusion.7
  195.9 0.0 copy-done.2
  195.9 0.0 copy-done.7
  195.9 0.0 copy-done.8
  195.9 4.2 %fusion.4 = bf16[1,512,2048]{2,1,0:T(8,128)(2,1)} fusion(bf16[1024,2048]{0,1:T(8,128)(2,1)S(1)} %bitcast.51, bf16[1024,512]{0,1:T(8,128)(2,1)S(1)} %add_convert_fusion, f32[1024]{0:T(1024)S(1)} %copy-done.7, f32[1024]{0:T(1024)S(1)} %copy-done.8, f32[512]{0:T(512)S(1)} %add_rsqrt_fusion, f32[512]{0:T(512)S(1)} %broadcast_multiply_fusion), kind=kOutput, calls=%fused_computation.34 | convolution fusion | flops 2153775104 | bytes 7352320 | tf_op jit(solution)/shard_map/ct,cr->tr/dot_general | solution.py:64
  (23 shorter events, 0.4 us)
Async XLA Ops:
  6.5 156.9 %copy-start = (bf16[1,512,2048]{2,1,0:T(8,128)(2,1)S(1)}, bf16[1,512,2048]{2,1,0:T(8,128)(2,1)}, u32[]{:S(2)}) copy-start(bf16[1,512,2048]{2,1,0:T(8,128)(2,1)} %param.9) | copy-start | bytes 6291460
  6.5 156.9 %all-gather.2.cloned.1.call-start = ((), (), s32[]{:S(2)}) async-start(), calls=%async_computation.1 | async-start | bytes 8912896 | tf_op jit(solution)/shard_map/all_gather | solution.py:16
  10.1 2.0 copy-start.1
  18.4 11.3 %copy-start.5 = (s32[1,512]{1,0:T(1,128)S(1)}, s32[1,512]{1,0:T(1,128)}, u32[]{:S(2)}) copy-start(s32[1,512]{1,0:T(1,128)} %param.10) | copy-start | bytes 6148
  18.4 12.6 %copy-start.3 = (f32[31,1024]{1,0:T(8,128)S(1)}, f32[31,1024]{1,0:T(8,128)}, u32[]{:S(2)}) copy-start(f32[31,1024]{1,0:T(8,128)} %param.14) | copy-start | bytes 380932
  18.4 154.3 %all-to-all-start = ((bf16[1024,16,128]{2,0,1:T(8,128)(2,1)}), bf16[1024,16,128]{2,0,1:T(8,128)(2,1)}, u32[]{:S(2)}, u32[]{:S(2)}) async-start(bf16[1024,16,128]{2,0,1:T(8,128)(2,1)} %copy.26), calls=%async_computation | async-start | bytes 8388608 | tf_op jit(solution)/shard_map/all_to_all | solution.py:11
  29.8 2.0 collective-permute-start
  163.4 4.7 %copy-start.6 = (bf16[2048,2048]{1,0:T(8,128)(2,1)S(1)}, bf16[2048,2048]{1,0:T(8,128)(2,1)}, u32[]{:S(2)}) copy-start(bf16[2048,2048]{1,0:T(8,128)(2,1)} %all-gather.2.cloned.1.call-done) | copy-start | bytes 25165828
  170.5 8.6 %collective-permute-start.1 = (bf16[1024,30]{0,1:T(8,128)(2,1)S(1)}, bf16[1024,30]{0,1:T(8,128)(2,1)S(1)}, u32[]{:S(2)}, u32[]{:S(2)}) collective-permute-start(bf16[1024,30]{0,1:T(8,128)(2,1)S(1)} %slice.351), channel_id=1, source_target_pairs={{0,16},{16,32},{32,48},{48,64},{64,80},{80,96},{96,112},{112,128},... | collective-permute-start | bytes 184328 | tf_op jit(solution)/shard_map/ppermute | solution.py:26
  172.7 6.4 %copy-start.4 = (f32[1024]{0:T(1024)S(1)}, f32[1024]{0:T(1024)}, u32[]{:S(2)}) copy-start(f32[1024]{0:T(1024)} %param.15) | copy-start | bytes 12292
  179.1 16.8 %copy-start.2 = (bf16[1024,16,128]{0,2,1:T(8,128)(2,1)S(1)}, bf16[1024,16,128]{0,2,1:T(8,128)(2,1)}, u32[]{:S(2)}) copy-start(bf16[1024,16,128]{0,2,1:T(8,128)(2,1)} %copy.27) | copy-start | bytes 12582916
  179.1 16.8 %copy-start.7 = (f32[1024]{0:T(1024)S(1)}, f32[1024]{0:T(1024)}, u32[]{:S(2)}) copy-start(f32[1024]{0:T(1024)} %param.17) | copy-start | bytes 12292
  179.1 16.8 %copy-start.8 = (f32[1024]{0:T(1024)S(1)}, f32[1024]{0:T(1024)}, u32[]{:S(2)}) copy-start(f32[1024]{0:T(1024)} %param.16) | copy-start | bytes 12292
Sparse Core Ops, SparseCore 0:
  9.5 153.9 all-gather.1
